TPU v7x, 32 devices: a whole 2x2x4 slice. The times are simulated.
32 devices in a mesh: sp: 4 (over z), dp: 8 (over y, x, core).
Axes of the slice: x: 2, y: 2, z: 4, core: 2. Of those that a mesh axis runs over, the one named last changes fastest.
Arguments:
- cotangent: bfloat16 [8, 512, 2048], P('dp', 'sp'), may hold values from -6 to 6
- unit_pre: bfloat16 [8, 512, 2048], P('dp', None, 'sp'), may hold values from -6 to 6
- gate_pre: bfloat16 [8, 512, 2048], P('dp', None, 'sp'), may hold values from -15 to 15
- out_weight: bfloat16 [2048, 2048], P('dp', 'sp'), may hold values from -0.125 to 0.125
- mix_weight: bfloat16 [8, 128, 128], replicated, may hold values from -0.5 to 0.5
- mix_bias: bfloat16 [8, 128], replicated, may hold values from 0.099609375 to 1.8984375
- norm_gain: bfloat16 [2048], P('sp'), may hold values from 0.099609375 to 1.8984375
- norm_shift: bfloat16 [2048], P('sp'), may hold values from -3 to 3
Outputs:
- unit_grad: bfloat16 [8, 512, 2048], P('dp', None, 'sp')
- gate_grad: bfloat16 [8, 512, 2048], P('dp', None, 'sp')
- out_weight_grad: float32 [2048, 2048], P('dp', 'sp')
- mix_weight_grad: float32 [8, 128, 128], replicated
- mix_bias_grad: float32 [8, 128], replicated
- gain_grad: float32 [2048], P('sp')
- shift_grad: float32 [2048], P('sp')
All inputs are finite; a program needn't handle non-finite values.
Results may differ from a plain program's by a relative error of at most 0.015.
Values may be sent and summed in bfloat16 or wider, within the bound.
No kernel may reach another device: no remote copies, remote signals or barrier semaphores. Data moves between devices by JAX's collectives and lax.ppermute only.
A program may use at most 64 MiB of HBM per device.

v0:
```python
import math
import jax
import jax.numpy as jnp
from jax import lax
from jax.sharding import PartitionSpec as P

GW = 2048
GROUPS = 8
BLK = 128
epsilon = 1e-05
tanh_coef = math.sqrt(2.0 / math.pi)


def gelu_slope(values):
    inner = tanh_coef * (values + 0.044715 * values * values * values)
    hyper = jnp.tanh(inner)
    return 0.5 * (1.0 + hyper) + 0.5 * values * (1.0 - hyper * hyper) * tanh_coef * (
        1.0 + 3.0 * 0.044715 * values * values
    )


def local(cotangent, unit_pre, gate_pre, out_weight, mix_weight, mix_bias, norm_gain, norm_shift):
    seq_len = unit_pre.shape[1]
    channels = unit_pre.shape[2]
    group_dim = GW // GROUPS
    span_width = min(channels, group_dim)
    groups_here = channels // span_width
    blocks = seq_len // BLK
    group_start = lax.axis_index("sp") * channels // group_dim
    units = unit_pre[0].astype(jnp.float32)
    gates = gate_pre[0].astype(jnp.float32)
    unit_act = jax.nn.gelu(units)
    gate_act = jax.nn.gelu(gates)
    moments = lax.psum((jnp.sum(gate_act, axis=-1), jnp.sum(gate_act * gate_act, axis=-1)), "sp")
    mean_val = moments[0] / GW
    var_val = moments[1] / GW - mean_val * mean_val
    rstd_val = lax.rsqrt(var_val + epsilon)
    centred = (gate_act - mean_val[:, None]) * rstd_val[:, None]
    gain_vec = norm_gain.astype(jnp.float32)
    normed = (centred * gain_vec + norm_shift.astype(jnp.float32)).astype(jnp.bfloat16)
    causal = jnp.arange(BLK)[:, None] >= jnp.arange(BLK)[None, :]
    local_weight = lax.dynamic_slice_in_dim(mix_weight, group_start, groups_here, 0)
    masked = jnp.where(causal[None], local_weight, jnp.zeros_like(local_weight))
    local_bias = lax.dynamic_slice_in_dim(mix_bias, group_start, groups_here, 0).astype(jnp.float32)
    normed_blocks = normed.reshape(blocks, BLK, groups_here, span_width)
    mixed = jnp.einsum("gts,nsgd->ntgd", masked, normed_blocks, preferred_element_type=jnp.float32)
    mixed = (mixed + local_bias.T[None, :, :, None]).reshape(seq_len, channels)
    gated = (unit_act * mixed).astype(jnp.bfloat16)
    weight_whole = lax.all_gather(out_weight, "dp", axis=0, tiled=True)
    dy_rows = lax.all_gather(cotangent, "sp", axis=1, tiled=True)[0]
    product = jnp.dot(dy_rows, weight_whole, preferred_element_type=jnp.float32)
    weight_part = lax.dot_general(
        dy_rows, gated, (((0,), (0,)), ((), ())), preferred_element_type=jnp.float32
    )
    token_count = lax.axis_size("dp") * seq_len
    norm_scale = 1.0 / math.sqrt(token_count)
    mix_scale = 1.0 / math.sqrt(token_count // BLK * group_dim)
    out_grad = (
        lax.psum_scatter(
            weight_part.astype(jnp.bfloat16), "dp", scatter_dimension=0, tiled=True
        ).astype(jnp.float32)
        * norm_scale
    )
    unit_grad = (product * mixed * gelu_slope(units)).astype(jnp.bfloat16)
    mix_grad = product * unit_act
    mix_round = mix_grad.astype(jnp.bfloat16).reshape(blocks, BLK, groups_here, span_width)
    mix_term = jnp.einsum(
        "ntgd,nsgd->gts", mix_round, normed_blocks, preferred_element_type=jnp.float32
    )
    mix_term = jnp.where(causal[None], mix_term, jnp.float32(0.0))
    bias_term = jnp.sum(mix_grad.reshape(blocks, BLK, groups_here, span_width), axis=(0, 3)).T
    normed_grad = jnp.einsum(
        "gts,ntgd->nsgd", masked, mix_round, preferred_element_type=jnp.float32
    ).reshape(seq_len, channels)
    gain_term = jnp.sum(normed_grad * centred, axis=0)
    shift_term = jnp.sum(normed_grad, axis=0)
    scaled = normed_grad * gain_vec
    back_sums = lax.psum((jnp.sum(scaled, axis=-1), jnp.sum(scaled * centred, axis=-1)), "sp")
    first_m = back_sums[0] / GW
    second_m = back_sums[1] / GW
    gate_grad = (
        rstd_val[:, None]
        * (scaled - first_m[:, None] - centred * second_m[:, None])
        * gelu_slope(gates)
    ).astype(jnp.bfloat16)
    empty_weight = jnp.zeros((GROUPS, BLK, BLK), jnp.float32)
    empty_bias = jnp.zeros((GROUPS, BLK), jnp.float32)
    mix_local, bias_local, gain_total, shift_total = (
        lax.psum(mix_term.astype(jnp.bfloat16), "dp").astype(jnp.float32),
        lax.psum(bias_term.astype(jnp.bfloat16), "dp").astype(jnp.float32),
        lax.psum(gain_term.astype(jnp.bfloat16), "dp").astype(jnp.float32),
        lax.psum(shift_term.astype(jnp.bfloat16), "dp").astype(jnp.float32),
    )
    full_weight = lax.dynamic_update_slice_in_dim(empty_weight, mix_local, group_start, 0)
    full_bias = lax.dynamic_update_slice_in_dim(empty_bias, bias_local, group_start, 0)
    full_weight, full_bias = (
        lax.psum(full_weight.astype(jnp.bfloat16), "sp").astype(jnp.float32),
        lax.psum(full_bias.astype(jnp.bfloat16), "sp").astype(jnp.float32),
    )
    return (
        unit_grad[None],
        gate_grad[None],
        out_grad,
        full_weight * mix_scale,
        full_bias * mix_scale,
        gain_total * norm_scale,
        shift_total * norm_scale,
    )


def solution(mesh):
    in_specs = (
        P("dp", "sp", None),
        P("dp", None, "sp"),
        P("dp", None, "sp"),
        P("dp", "sp"),
        P(),
        P(),
        P("sp"),
        P("sp"),
    )
    out_specs = (
        P("dp", None, "sp"),
        P("dp", None, "sp"),
        P("dp", "sp"),
        P(),
        P(),
        P("sp"),
        P("sp"),
    )
    return jax.shard_map(local, mesh=mesh, in_specs=in_specs, out_specs=out_specs, check_vma=False)
```

profile of v0, /device:TPU:0, one launch (start us, length us, event | category | flops | bytes accessed | tf_op | source)
XLA Modules:
  0.0 237.9 jit_solution(5552104702866696244)
XLA Ops:
  7.2 0.0 all-gather.3.cloned.1.call-start
  7.2 0.7 all-gather.3.cloned.1.call-update
  7.9 0.0 all-gather.5.cloned.1.call-start
  8.0 0.7 all-gather.5.cloned.1.call-update
  8.7 0.0 all-reduce.6.cloned.1.call-start
  8.7 1.7 reshape.181
  10.4 0.5 copy.70
  11.0 0.6 reshape.185
  11.7 1.3 copy.78
  13.0 0.5 fusion.70
  13.5 13.9 %all-reduce.1 = (f32[512]{0:T(512)S(1)}, f32[512]{0:T(512)S(1)}) all-reduce(f32[512]{0:T(512)S(1)} %get-tuple-element.40, f32[512]{0:T(512)S(1)} %get-tuple-element.39), channel_id=1, replica_groups=mesh['sp'=4,'dp'=8] {'sp'}, use_global_device_ids=true, to_apply=%region_3.4 | all-reduce | flops 1024 | bytes 8192 | tf_op jit(solution)/shard_map/psum | solution.py:34
  27.5 0.7 convert_bitcast_fusion.1
  28.2 3.3 %fusion.43 = (bf16[4,128,2,256]{1,3,0,2:T(8,128)(2,1)}, f32[4,128,2,256]{1,3,0,2:T(8,128)}) fusion(f32[4,128,2,256]{1,3,0,2:T(8,128)} %copy.78, f32[128,2]{0,1:T(2,128)S(1)} %convert_bitcast_fusion.1, bf16[8,128,128]{2,1,0:T(8,128)(2,1)S(1)} %copy-done.7, s32[]{:T(128)S(6)} %select_n.20, pred[128,128]{1,0:T(8,128)(4,1)S(1)} %iota_compare_fusion, ...), kind=kOutput, calls=%fused_computation.64 | convolution fusion | flops 73433088 | bytes 3761156 | tf_op jit(solution)/shard_map/gts,nsgd->ntgd/dot_general | solution.py:46
  31.5 1.5 copy.71
  33.0 1.0 copy.87
  34.1 24.0 %all-gather.3.cloned.1.call-done = bf16[1,512,2048]{2,1,0:T(8,128)(2,1)} async-done(((bf16[1,128,2048]{2,1,0:T(8,128)(2,1)}), bf16[1,512,2048]{2,1,0:T(8,128)(2,1)}) %all-gather.3.cloned.1.call-update) | async-done | bytes 2097168 | tf_op jit(solution)/shard_map/all_gather | solution.py:50
  58.0 28.5 %all-gather.5.cloned.1.call-done = bf16[2048,512]{1,0:T(8,128)(2,1)} async-done(((bf16[256,512]{1,0:T(8,128)(2,1)}), bf16[2048,512]{1,0:T(8,128)(2,1)}) %all-gather.5.cloned.1.call-update) | async-done | bytes 2097168 | tf_op jit(solution)/shard_map/all_gather | solution.py:49
  86.6 5.6 %fusion.85 = (bf16[512,512]{1,0:T(8,128)(2,1)}, f32[512,512]{1,0:T(8,128)S(1)}, bf16[1,512,512]{2,1,0:T(8,128)(2,1)}) fusion(bf16[1,512,512]{2,1,0:T(8,128)(2,1)S(1)} %copy-done.2, f32[512,512]{1,0:T(8,128)} %bitcast.107, bf16[2048,512]{1,0:T(8,128)(2,1)} %all-gather.5.cloned.1.call-done, bf16[1,512,2048]{2,1,0:T(8,128)(2,1)} %all-gather.3.cloned.1.call-done), kind=kOutput, calls=%fused_computation.126 | convolution fusion | flops 1081868288 | bytes 7864320 | tf_op jit(solution)/shard_map/dot_general | solution.py:51
  92.2 1.2 reshape.178
  93.3 1.4 fusion.10
  94.7 0.0 all-reduce.6.cloned.1.call-update
  94.7 0.0 all-reduce.8.cloned.1.call-start
  94.8 1.4 copy.79
  96.2 0.9 copy.88
  97.1 51.0 %all-reduce.6.cloned.1.call-done = bf16[2,128,128]{2,1,0:T(8,128)(2,1)} async-done(((bf16[2,128,128]{2,1,0:T(8,128)(2,1)}), bf16[2,128,128]{2,1,0:T(8,128)(2,1)}) %all-reduce.6.cloned.1.call-update) | async-done | bytes 65552 | tf_op jit(solution)/shard_map/psum | solution.py:89
  148.1 0.9 convert_dynamic-update-slice_fusion
  149.0 0.7 copy-done.1
  149.7 0.0 all-reduce.8.cloned.1.call-update
  149.7 0.0 reduce-scatter.2.cloned.1.call-start
  149.7 4.3 %fusion = bf16[2048,512]{0,1:T(8,128)(2,1)} fusion(bf16[512,512]{1,0:T(8,128)(2,1)} %bitcast.108, bf16[1,512,2048]{2,1,0:T(8,128)(2,1)} %all-gather.3.cloned.1.call-done), kind=kOutput, calls=%fused_computation.13 | convolution fusion | flops 1074790400 | bytes 4718592 | tf_op jit(solution)/shard_map/dot_general | solution.py:52
  154.1 1.0 copy-done.4
  155.1 1.8 multiply_reduce_fusion
  156.9 0.7 reshape.180
  157.6 0.4 reduce_sum.73
  158.0 0.1 copy.91
  158.1 1.6 copy.73
  159.6 0.8 reshape.179
  160.5 11.8 %all-reduce.2 = (bf16[2,128]{1,0:T(2,128)(2,1)S(1)}, bf16[512]{0:T(512)(128)(2,1)S(1)}, bf16[512]{0:T(512)(128)(2,1)S(1)}) all-reduce(bf16[2,128]{1,0:T(2,128)(2,1)S(1)} %bitcast.114, bf16[512]{0:T(512)(128)(2,1)S(1)} %bitcast.112, bf16[512]{0:T(512)(128)(2,1)S(1)} %bitcast.113), channel_id=1, replica_groups=mesh['sp'=4,'dp'=8] {'dp'}, use_global_device_ids=true, to_apply=%region_12.13 | all-reduce | flops 1280 | bytes 5120 | tf_op jit(solution)/shard_map/psum | solution.py:90
  172.3 0.1 dynamic_update_slice.7
  172.4 12.0 %psum.77 = bf16[8,128]{1,0:T(8,128)(2,1)S(1)} all-reduce(bf16[8,128]{1,0:T(8,128)(2,1)S(1)} %dynamic_update_slice.7), channel_id=1, replica_groups=mesh['sp'=4,'dp'=8] {'sp'}, use_global_device_ids=true, to_apply=%region_13.14 | all-reduce | flops 1024 | bytes 4096 | tf_op jit(solution)/shard_map/psum | solution.py:98
  184.4 8.4 %all-reduce = (f32[512]{0:T(512)S(1)}, f32[512]{0:T(512)S(1)}) all-reduce(f32[512]{0:T(512)S(1)} %bitcast.115, f32[512]{0:T(512)S(1)} %bitcast.116), channel_id=1, replica_groups=mesh['sp'=4,'dp'=8] {'sp'}, use_global_device_ids=true, to_apply=%region_7.8 | all-reduce | flops 1024 | bytes 8192 | tf_op jit(solution)/shard_map/psum | solution.py:78
  192.7 0.6 convert_multiply_fusion.11
  193.3 0.6 convert_multiply_fusion.12
  193.9 2.1 fusion.69
  196.1 1.8 convert_multiply_fusion.9
  197.9 31.5 %reduce-scatter.2.cloned.1.call-done = bf16[256,512]{0,1:T(8,128)(2,1)} async-done(((bf16[2048,512]{0,1:T(8,128)(2,1)}), bf16[256,512]{0,1:T(8,128)(2,1)}) %reduce-scatter.2.cloned.1.call-update) | async-done | bytes 262160 | tf_op jit(solution)/shard_map/reduce_scatter | solution.py:59
  229.4 1.0 convert_multiply_fusion.10
  230.4 1.0 copy.83
  (26 shorter events, 0.2 us)
Async XLA Ops:
  7.2 50.9 %all-gather.3.cloned.1.call-start = ((), (), s32[]{:S(2)}) async-start(), calls=%async_computation.1 | async-start | bytes 2621440 | tf_op jit(solution)/shard_map/all_gather | solution.py:50
  7.9 3.0 %copy-start.5 = (bf16[512]{0:T(512)(128)(2,1)S(1)}, bf16[512]{0:T(512)(128)(2,1)}, u32[]{:S(2)}) copy-start(bf16[512]{0:T(512)(128)(2,1)} %param.14) | copy-start | bytes 3076
  7.9 3.1 %copy-start.6 = (bf16[512]{0:T(512)(128)(2,1)S(1)}, bf16[512]{0:T(512)(128)(2,1)}, u32[]{:S(2)}) copy-start(bf16[512]{0:T(512)(128)(2,1)} %param.15) | copy-start | bytes 3076
  7.9 3.1 %copy-start.2 = (bf16[1,512,512]{2,1,0:T(8,128)(2,1)S(1)}, bf16[1,512,512]{2,1,0:T(8,128)(2,1)}, u32[]{:S(2)}) copy-start(bf16[1,512,512]{2,1,0:T(8,128)(2,1)} %param.9) | copy-start | bytes 1572868
  7.9 78.7 %all-gather.5.cloned.1.call-start = ((), (), s32[]{:S(2)}) async-start(), calls=%async_computation.2 | async-start | bytes 2359296 | tf_op jit(solution)/shard_map/all_gather | solution.py:49
  8.7 139.4 %all-reduce.6.cloned.1.call-start = ((), (), s32[]{:S(2)}) async-start(), calls=%async_computation.4 | async-start | bytes 131072 | tf_op jit(solution)/shard_map/psum | solution.py:89
  11.0 2.0 copy-start
  11.0 17.2 %copy-start.7 = (bf16[8,128,128]{2,1,0:T(8,128)(2,1)S(1)}, bf16[8,128,128]{2,1,0:T(8,128)(2,1)}, u32[]{:S(2)}) copy-start(bf16[8,128,128]{2,1,0:T(8,128)(2,1)} %param.12) | copy-start | bytes 786436
  93.3 1.4 copy-start.3
  94.7 101.3 %all-reduce.8.cloned.1.call-start = ((), (), s32[]{:S(2)}) async-start(), calls=%async_computation.5 | async-start | bytes 524288 | tf_op jit(solution)/shard_map/psum | solution.py:97
  149.0 0.7 copy-start.1
  149.7 79.7 %reduce-scatter.2.cloned.1.call-start = ((), (), s32[]{:S(2)}) async-start(), calls=%async_computation.3 | async-start | bytes 2359296 | tf_op jit(solution)/shard_map/reduce_scatter | solution.py:59
  154.1 1.1 copy-start.4
Sparse Core Ops, SparseCore 0:
  9.5 48.4 all-gather.2
  59.9 26.6 all-gather.4
  94.9 53.1 all-reduce.5
  150.3 35.0 all-reduce.7
  188.4 40.9 reduce-scatter.1
where the time goes:
time: 238 us
  waiting for transfers between devices  136 us (57%)
  blocking collectives  46.1 us (19%)
  matrix products  16.3 us (7%)
  local copies, waits for them, and re-layouts  16.2 us (7%)
  between operations  14 us (6%)
  other arithmetic  8.61 us (4%)
    psum x1, waiting for transfers between devices, local(): lax.psum(mix_term.astype(jnp.bfloat16), 'dp').astype(jnp.float32)  51 us
    reduce_scatter x1, waiting for transfers between devices, local(): lax.psum_scatter(weight_part.astype(jnp.bfloat16), 'dp', scatter_dimensio...  31.5 us
    all_gather x1, waiting for transfers between devices, local(): weight_whole = lax.all_gather(out_weight, 'dp', axis=0, tiled=True)  28.5 us
    all_gather x1, waiting for transfers between devices, local(): dy_rows = lax.all_gather(cotangent, 'sp', axis=1, tiled=True)[0]  24 us
    psum x1, blocking collectives, local(): lax.psum((jnp.sum(gate_act, axis=-1), jnp.sum(gate_act * gate_act, axis=-...  13.9 us
    psum x1, blocking collectives, local(): lax.psum(full_bias.astype(jnp.bfloat16), 'sp').astype(jnp.float32)  12 us
    psum x1, blocking collectives, local(): lax.psum(bias_term.astype(jnp.bfloat16), 'dp').astype(jnp.float32)  11.8 us
    psum x1, blocking collectives, local(): lax.psum((jnp.sum(scaled, axis=-1), jnp.sum(scaled * centred, axis=-1)),...  8.36 us
  transfers between devices with their start and end apart: 5, of which 4 were waited for; matrix products, arithmetic and copies ran while one was open for 12% of the time, Pallas kernels for 0%

commit v1 on v0

--- a/solution.py
+++ b/solution.py
@@ -85,8 +85,13 @@
     ).astype(jnp.bfloat16)
     empty_weight = jnp.zeros((GROUPS, BLK, BLK), jnp.float32)
     empty_bias = jnp.zeros((GROUPS, BLK), jnp.float32)
+
+    def shape_sums_all_on_mesh(original, net_axis):
+        step_out = jnp.sum(lax.all_gather(original, axis_name=net_axis), axis=0)
+        return step_out
+
     mix_local, bias_local, gain_total, shift_total = (
-        lax.psum(mix_term.astype(jnp.bfloat16), "dp").astype(jnp.float32),
+        shape_sums_all_on_mesh(mix_term.astype(jnp.bfloat16), "dp").astype(jnp.float32),
         lax.psum(bias_term.astype(jnp.bfloat16), "dp").astype(jnp.float32),
         lax.psum(gain_term.astype(jnp.bfloat16), "dp").astype(jnp.float32),
         lax.psum(shift_term.astype(jnp.bfloat16), "dp").astype(jnp.float32),

time: 238 us -> 195 us (0.82)
  waiting for transfers between devices: 136 us -> 82.2 us
  blocking collectives: 46.1 us -> 57 us
    psum x1 -> x0, waiting for transfers between devices: 51 us -> none  [local(): lax.psum(mix_term.astype(jnp.bfloat16), 'dp').astype(jnp.float32)]
    all_gather x0 -> x1, blocking collectives: none -> 9.82 us  [shape_sums_all_on_mesh(): step_out = jnp.sum(lax.all_gather(original, axis_name=net_axis), axis=0)]
  transfers between devices with their start and end apart: 5 -> 4, of which waited for: 4 -> 3; matrix products, arithmetic and copies ran while one was open for 12% -> 15% of each run, Pallas kernels for 0% -> 0%
where the time goes in v1:
time: 195 us; the launch traced here: 194 us
  waiting for transfers between devices  82.2 us (42%)
  blocking collectives  57 us (29%)
  local copies, waits for them, and re-layouts  17 us (9%)
  matrix products  15.7 us (8%)
  between operations  14 us (7%)
  other arithmetic  7.81 us (4%)
    reduce_scatter x1, waiting for transfers between devices, local(): lax.psum_scatter(weight_part.astype(jnp.bfloat16), 'dp', scatter_dimensio...  30.5 us
    all_gather x1, waiting for transfers between devices, local(): weight_whole = lax.all_gather(out_weight, 'dp', axis=0, tiled=True)  28.5 us
    all_gather x1, waiting for transfers between devices, local(): dy_rows = lax.all_gather(cotangent, 'sp', axis=1, tiled=True)[0]  21.7 us
    psum x1, blocking collectives, local(): lax.psum((jnp.sum(gate_act, axis=-1), jnp.sum(gate_act * gate_act, axis=-...  13.9 us
    psum x1, blocking collectives, local(): lax.psum(bias_term.astype(jnp.bfloat16), 'dp').astype(jnp.float32)  13.6 us
    psum x1, blocking collectives, local(): lax.psum(full_bias.astype(jnp.bfloat16), 'sp').astype(jnp.float32)  11.3 us
    all_gather x1, blocking collectives, shape_sums_all_on_mesh(): step_out = jnp.sum(lax.all_gather(original, axis_name=net_axis), axis=0)  9.82 us
    psum x1, blocking collectives, local(): lax.psum((jnp.sum(scaled, axis=-1), jnp.sum(scaled * centred, axis=-1)),...  8.39 us
  transfers between devices with their start and end apart: 4, of which 3 were waited for; matrix products, arithmetic and copies ran while one was open for 15% of the time, Pallas kernels for 0%

profile of v1, /device:TPU:0, one launch (start us, length us, event | category | flops | bytes accessed | tf_op | source)
XLA Modules:
  0.0 194.1 jit_solution(13900895700849009858)
XLA Ops:
  7.2 0.0 all-gather.4.cloned.1.call-start
  7.2 0.7 all-gather.4.cloned.1.call-update
  7.9 0.0 all-gather.6.cloned.1.call-start
  8.0 0.7 all-gather.6.cloned.1.call-update
  8.7 0.0 all-reduce.5.cloned.1.call-start
  8.7 1.7 reshape.181
  10.4 0.5 copy.70
  11.0 0.6 reshape.185
  11.7 1.3 copy.78
  13.0 0.5 fusion.70
  13.5 13.9 %all-reduce.1 = (f32[512]{0:T(512)S(1)}, f32[512]{0:T(512)S(1)}) all-reduce(f32[512]{0:T(512)S(1)} %get-tuple-element.40, f32[512]{0:T(512)S(1)} %get-tuple-element.39), channel_id=1, replica_groups=mesh['sp'=4,'dp'=8] {'sp'}, use_global_device_ids=true, to_apply=%region_3.4 | all-reduce | flops 1024 | bytes 8192 | tf_op jit(solution)/shard_map/psum | solution.py:34
  27.5 0.7 convert_bitcast_fusion.1
  28.2 3.3 %fusion.43 = (bf16[4,128,2,256]{1,3,0,2:T(8,128)(2,1)}, f32[4,128,2,256]{1,3,0,2:T(8,128)}) fusion(f32[4,128,2,256]{1,3,0,2:T(8,128)} %copy.78, f32[128,2]{0,1:T(2,128)S(1)} %convert_bitcast_fusion.1, bf16[8,128,128]{2,1,0:T(8,128)(2,1)S(1)} %copy-done.7, s32[]{:T(128)S(6)} %select_n.20, pred[128,128]{1,0:T(8,128)(4,1)S(1)} %iota_compare_fusion, ...), kind=kOutput, calls=%fused_computation.64 | convolution fusion | flops 73433088 | bytes 3761156 | tf_op jit(solution)/shard_map/gts,nsgd->ntgd/dot_general | solution.py:46
  31.5 1.5 copy.71
  33.0 1.0 copy.87
  34.1 1.4 copy.79
  35.5 0.9 copy.88
  36.3 21.7 %all-gather.4.cloned.1.call-done = bf16[1,512,2048]{2,1,0:T(8,128)(2,1)} async-done(((bf16[1,128,2048]{2,1,0:T(8,128)(2,1)}), bf16[1,512,2048]{2,1,0:T(8,128)(2,1)}) %all-gather.4.cloned.1.call-update) | async-done | bytes 2097168 | tf_op jit(solution)/shard_map/all_gather | solution.py:50
  58.0 28.5 %all-gather.6.cloned.1.call-done = bf16[2048,512]{1,0:T(8,128)(2,1)} async-done(((bf16[256,512]{1,0:T(8,128)(2,1)}), bf16[2048,512]{1,0:T(8,128)(2,1)}) %all-gather.6.cloned.1.call-update) | async-done | bytes 2097168 | tf_op jit(solution)/shard_map/all_gather | solution.py:49
  86.6 5.6 %fusion.85 = (bf16[512,512]{1,0:T(8,128)(2,1)}, f32[512,512]{1,0:T(8,128)S(1)}, bf16[1,512,512]{2,1,0:T(8,128)(2,1)}) fusion(bf16[1,512,512]{2,1,0:T(8,128)(2,1)S(1)} %copy-done.2, f32[512,512]{1,0:T(8,128)} %bitcast.109, bf16[2048,512]{1,0:T(8,128)(2,1)} %all-gather.6.cloned.1.call-done, bf16[1,512,2048]{2,1,0:T(8,128)(2,1)} %all-gather.4.cloned.1.call-done), kind=kOutput, calls=%fused_computation.126 | convolution fusion | flops 1081868288 | bytes 7864320 | tf_op jit(solution)/shard_map/dot_general | solution.py:51
  92.2 1.2 reshape.178
  93.3 0.8 copy-done.3
  94.1 0.7 fusion.10
  94.9 9.8 %all-gather = bf16[16,128,128]{2,1,0:T(8,128)(2,1)S(1)} all-gather(bf16[2,128,128]{2,1,0:T(8,128)(2,1)S(1)} %fusion.10), channel_id=2, replica_groups=mesh['sp'=4,'dp'=8] {'dp'}, dimensions={0}, use_global_device_ids=true | all-gather | bytes 589824 | tf_op jit(solution)/shard_map/all_gather | solution.py:90
  104.7 0.1 reduce_sum.85
  104.8 0.7 copy-done.1
  105.5 0.0 all-reduce.5.cloned.1.call-update
  105.6 0.2 reduce-scatter.2.cloned.1.call-start
  105.8 4.3 %fusion = bf16[2048,512]{0,1:T(8,128)(2,1)} fusion(bf16[512,512]{1,0:T(8,128)(2,1)} %bitcast.110, bf16[1,512,2048]{2,1,0:T(8,128)(2,1)} %all-gather.4.cloned.1.call-done), kind=kOutput, calls=%fused_computation.13 | convolution fusion | flops 1074790400 | bytes 4718592 | tf_op jit(solution)/shard_map/dot_general | solution.py:52
  110.1 0.0 reduce-scatter.2.cloned.1.call-update
  110.2 1.0 copy-done.4
  111.2 1.8 multiply_reduce_fusion
  113.0 0.7 reshape.180
  113.6 0.4 reduce_sum.86
  114.0 0.1 copy.91
  114.1 1.6 copy.73
  115.7 0.8 reshape.179
  116.5 13.6 %all-reduce.2 = (bf16[2,128]{1,0:T(2,128)(2,1)S(1)}, bf16[512]{0:T(512)(128)(2,1)S(1)}, bf16[512]{0:T(512)(128)(2,1)S(1)}) all-reduce(bf16[2,128]{1,0:T(2,128)(2,1)S(1)} %bitcast.116, bf16[512]{0:T(512)(128)(2,1)S(1)} %bitcast.114, bf16[512]{0:T(512)(128)(2,1)S(1)} %bitcast.115), channel_id=1, replica_groups=mesh['sp'=4,'dp'=8] {'dp'}, use_global_device_ids=true, to_apply=%region_12.13 | all-reduce | flops 1280 | bytes 5120 | tf_op jit(solution)/shard_map/psum | solution.py:95
  130.1 0.1 dynamic_update_slice.7
  130.2 11.3 %psum.69 = bf16[8,128]{1,0:T(8,128)(2,1)S(1)} all-reduce(bf16[8,128]{1,0:T(8,128)(2,1)S(1)} %dynamic_update_slice.7), channel_id=1, replica_groups=mesh['sp'=4,'dp'=8] {'sp'}, use_global_device_ids=true, to_apply=%region_13.14 | all-reduce | flops 1024 | bytes 4096 | tf_op jit(solution)/shard_map/psum | solution.py:103
  141.5 8.4 %all-reduce = (f32[512]{0:T(512)S(1)}, f32[512]{0:T(512)S(1)}) all-reduce(f32[512]{0:T(512)S(1)} %bitcast.117, f32[512]{0:T(512)S(1)} %bitcast.118), channel_id=1, replica_groups=mesh['sp'=4,'dp'=8] {'sp'}, use_global_device_ids=true, to_apply=%region_7.8 | all-reduce | flops 1024 | bytes 8192 | tf_op jit(solution)/shard_map/psum | solution.py:78
  149.9 0.6 convert_multiply_fusion.11
  150.5 0.6 convert_multiply_fusion.12
  151.1 2.1 %fusion.69 = bf16[1,512,512]{2,1,0:T(8,128)(2,1)} fusion(bf16[1,512,512]{2,1,0:T(8,128)(2,1)S(1)} %copy-done, f32[1,512,512]{2,1,0:T(8,128)S(1)} %reshape.179, f32[512]{0:T(512)S(1)} %get-tuple-element.57, f32[512]{0:T(512)S(1)} %get-tuple-element.51, f32[512]{0:T(512)S(1)} %get-tuple-element.58, f32[512]{0:T(512)S(1)} %convert_element_type.114, ...), kind=kLoop, calls=%fused_computation.95 | loop fusion | flops 9175040 | bytes 2107392 | tf_op jit(solution)/shard_map/convert_element_type | solution.py:85
  153.2 1.8 convert_multiply_fusion.9
  155.0 30.5 %reduce-scatter.2.cloned.1.call-done = bf16[256,512]{0,1:T(8,128)(2,1)} async-done(((bf16[2048,512]{0,1:T(8,128)(2,1)}), bf16[256,512]{0,1:T(8,128)(2,1)}) %reduce-scatter.2.cloned.1.call-update) | async-done | bytes 262160 | tf_op jit(solution)/shard_map/reduce_scatter | solution.py:59
  185.6 1.0 convert_multiply_fusion.10
  186.5 1.0 copy.83
  (25 shorter events, 0.2 us)
Async XLA Ops:
  7.2 50.9 %all-gather.4.cloned.1.call-start = ((), (), s32[]{:S(2)}) async-start(), calls=%async_computation.1 | async-start | bytes 2621440 | tf_op jit(solution)/shard_map/all_gather | solution.py:50
  7.9 3.0 %copy-start.5 = (bf16[512]{0:T(512)(128)(2,1)S(1)}, bf16[512]{0:T(512)(128)(2,1)}, u32[]{:S(2)}) copy-start(bf16[512]{0:T(512)(128)(2,1)} %param.14) | copy-start | bytes 3076
  7.9 3.1 %copy-start.6 = (bf16[512]{0:T(512)(128)(2,1)S(1)}, bf16[512]{0:T(512)(128)(2,1)}, u32[]{:S(2)}) copy-start(bf16[512]{0:T(512)(128)(2,1)} %param.15) | copy-start | bytes 3076
  7.9 3.1 %copy-start.2 = (bf16[1,512,512]{2,1,0:T(8,128)(2,1)S(1)}, bf16[1,512,512]{2,1,0:T(8,128)(2,1)}, u32[]{:S(2)}) copy-start(bf16[1,512,512]{2,1,0:T(8,128)(2,1)} %param.9) | copy-start | bytes 1572868
  7.9 78.7 %all-gather.6.cloned.1.call-start = ((), (), s32[]{:S(2)}) async-start(), calls=%async_computation.2 | async-start | bytes 2359296 | tf_op jit(solution)/shard_map/all_gather | solution.py:49
  8.7 144.6 %all-reduce.5.cloned.1.call-start = ((), (), s32[]{:S(2)}) async-start(), calls=%async_computation.4 | async-start | bytes 524288 | tf_op jit(solution)/shard_map/psum | solution.py:102
  11.0 2.0 %copy-start = (bf16[1,512,512]{2,1,0:T(8,128)(2,1)S(1)}, bf16[1,512,512]{2,1,0:T(8,128)(2,1)}, u32[]{:S(2)}) copy-start(bf16[1,512,512]{2,1,0:T(8,128)(2,1)} %param.10) | copy-start | bytes 1572868
  11.0 17.2 %copy-start.7 = (bf16[8,128,128]{2,1,0:T(8,128)(2,1)S(1)}, bf16[8,128,128]{2,1,0:T(8,128)(2,1)}, u32[]{:S(2)}) copy-start(bf16[8,128,128]{2,1,0:T(8,128)(2,1)} %param.12) | copy-start | bytes 786436
  93.3 0.8 copy-start.3
  104.8 0.7 copy-start.1
  105.6 80.0 %reduce-scatter.2.cloned.1.call-start = ((), (), s32[]{:S(2)}) async-start(), calls=%async_computation.3 | async-start | bytes 2359296 | tf_op jit(solution)/shard_map/reduce_scatter | solution.py:59
  110.1 1.1 copy-start.4
Sparse Core Ops, SparseCore 0:
  9.5 48.4 all-gather.3
  59.9 26.6 all-gather.5
  105.7 35.6 all-reduce.4
  144.5 40.9 reduce-scatter.1
